TPU v7x, 256 devices: a whole 4x4x8 slice. The times are simulated.
256 devices in a mesh: sp: 64 (over z, y, core), tp: 4 (over x).
Axes of the slice: x: 4, y: 4, z: 8, core: 2. Of those that a mesh axis runs over, the one named last changes fastest.
Arguments:
- residual: bfloat16 [12288, 2048], P(('sp', 'tp')), may hold values from -6 to 6
- mixer_input: bfloat16 [12288, 512], P('sp', 'tp'), may hold values from -6 to 6
- log_gate: float32 [12288, 32], P('sp', 'tp'), may hold values from -2 to 0
- decay_rate: float32 [2, 32, 64], P(None, 'tp'), may hold values from 0 to 1
- turn_rate: float32 [2, 32, 64], P(None, 'tp'), may hold values from -1 to 1
- drive_real: float32 [2, 32, 16, 64], P(None, 'tp'), may hold values from -1 to 1
- drive_imaginary: float32 [2, 32, 16, 64], P(None, 'tp'), may hold values from -1 to 1
- read_real: float32 [2, 32, 16, 64], P(None, 'tp'), may hold values from -0.75 to 0.75
- read_imaginary: float32 [2, 32, 16, 64], P(None, 'tp'), may hold values from -0.75 to 0.75
- skip_gain: float32 [512], P('tp'), may hold values from -4 to 4
- project_weight: bfloat16 [512, 2048], replicated, may hold values from -0.25 to 0.25
- norm_gain: float32 [2048], replicated, may hold values from 0.1 to 1.9
- final_gain: float32 [2048], replicated, may hold values from 0.1 to 1.9
- routes: int32 [12288, 2], P('sp'), may hold values from 0 to 63, all different within a row; in each aligned block of 48 rows (0 to 47, 48 to 95, ...) at most 2 rows name the same one
- group_weight: float32 [12288], P('sp'), may hold values from 0.2 to 1
- expert_weight: float32 [12288, 2], P('sp'), may hold values from 0.1 to 1
- gate_weight: bfloat16 [64, 2048, 1024], P('sp', None, 'tp'), may hold values from -0.125 to 0.125
- linear_weight: bfloat16 [64, 2048, 1024], P('sp', None, 'tp'), may hold values from -0.125 to 0.125
- down_weight: bfloat16 [64, 1024, 2048], P('sp', 'tp'), may hold values from -0.1875 to 0.1875
Outputs:
- finished: bfloat16 [12288, 2048], P(('sp', 'tp'))
Inputs may be any that keep to these rules, and one draw needn't show every extreme that they name: `routes`: each row names 2 different experts. In each aligned block of 48 rows no expert is named by more than 2 rows; some expert is named by exactly 2 rows of some block.
All inputs are finite; a program needn't handle non-finite values.
Results may differ from a plain program's by a relative error of at most 0.006.
Values may be sent and summed in bfloat16 or wider, within the bound.
A program may use at most 128 MiB of HBM per device.

v0:
```python
import jax
import jax.numpy as jnp
from jax import lax
from jax.experimental import pallas as pl
from jax.experimental.pallas import tpu as pltpu
from jax.sharding import PartitionSpec as P

MESH = pl.DeviceIdType.MESH
F32 = jnp.float32
BF16 = jnp.bfloat16
deep_alpha = 2.0**0.25
norm_epsilon = 1e-05
SEGMENT = 24
CHUNKS = 4
WIDE = 512


def iota(shape, dim):
    return lax.broadcasted_iota(jnp.int32, shape, dim)


def cmul(a, b):
    return (a[0] * b[0] - a[1] * b[1], a[0] * b[1] + a[1] * b[0])


def dot(a, b):
    return jnp.dot(a, b, preferred_element_type=F32)


def dot_nt(a, b):
    return lax.dot_general(a, b, (((1,), (1,)), ((), ())), preferred_element_type=F32)


def dot_tn(a, b):
    return lax.dot_general(a, b, (((0,), (0,)), ((), ())), preferred_element_type=F32)


def halves(value):
    high = value.astype(BF16)
    return high, (value - high.astype(F32)).astype(BF16)


def one_minus_exp_neg(x):
    series = x * (1.0 - x * (0.5 - x * (1.0 / 6 - x * (1.0 / 24 - x * (1.0 / 120 - x / 720)))))
    return jnp.where(x < 0.25, series, 1.0 - jnp.exp(-x))


def expand(value):
    both = jnp.concatenate([value, value], axis=1)
    row, lane = iota((8, 128), 0), iota((8, 128), 1)
    parts = [
        jnp.sum(jnp.where(row == 2 * q + (lane >= 64).astype(jnp.int32), both, 0.0), axis=0, keepdims=True)
        for q in range(4)
    ]
    return jnp.concatenate(parts, axis=1)


def inclusive(a, s, backward):
    row = iota(s[0].shape, 0)
    for shift in (1, 2, 4):
        ok = row < 8 - shift if backward else row >= shift
        turn = 8 - shift if backward else shift
        pa = tuple(pltpu.roll(v, turn, 0) for v in a)
        ps = tuple(pltpu.roll(v, turn, 0) for v in s)
        na, ns = cmul(a, pa), cmul(a, ps)
        s = tuple(jnp.where(ok, n + o, o) for n, o in zip(ns, s))
        a = tuple(jnp.where(ok, n, o) for n, o in zip(na, a))
    return a, s


def exclusive(a, s, backward):
    row = iota(s[0].shape, 0)
    ok = row < 7 if backward else row >= 1
    turn = 7 if backward else 1
    ident = (1.0, 0.0)
    ea = tuple(jnp.where(ok, pltpu.roll(v, turn, 0), i) for v, i in zip(a, ident))
    es = tuple(jnp.where(ok, pltpu.roll(v, turn, 0), 0.0) for v in s)
    return ea, es


def product(g):
    for shift in (1, 2, 4):
        g = g * pltpu.roll(g, shift, 0)
    return g


def pick(value, index):
    row = iota(value.shape, 0)
    return jnp.sum(jnp.where(row == index, value, 0.0), axis=0, keepdims=True)


def kernel(
    residual, mixer_input, log_gate, decay_rate, turn_rate, drive_real, drive_imag, read_real,
    read_imag, skip_gain, project_hbm, norm_gain, final_gain, routes, group_weight, expert_weight,
    gate_hbm, linear_hbm, down_hbm,
    out,
    project, w_gate, w_linear, w_down,
    gates, push, msg1, recv1, msg2, recv2, act_out, act_in, middle, rows,
    out1, in1, out2, xin, gate_acc, linear_acc, hidden,
    opp_out, fwd_r, fwd_l, right_out, left_out, from_l, from_r, keep_r, keep_l,
    ans, b2in, b2out, b1in,
    w_sem, small_send, small_recv, yc_send, yc_recv, z_send, z_recv, x_send, x_recv, o_recv,
    rs_send, rs_recv,
):
    sp, x = lax.axis_index("sp"), lax.axis_index("tp")
    z, yc = sp // 8, lax.rem(sp, 8)
    right, left, opposite = lax.rem(x + 1, 4), lax.rem(x + 3, 4), lax.rem(x + 2, 4)

    def yc_peer(k):
        other = lax.rem(yc + k, 8)
        return other, (z * 8 + other, x)

    def z_peer(k):
        other = lax.rem(z + k, 8)
        return other, (other * 8 + yc, x)

    def send(src, dst, s_sem, r_sem, device):
        pltpu.make_async_remote_copy(
            src_ref=src, dst_ref=dst, send_sem=s_sem, recv_sem=r_sem,
            device_id=device, device_id_type=MESH,
        ).start()

    def settle(ref, sem):
        pltpu.make_async_copy(ref, ref, sem).wait()

    barrier = pltpu.get_barrier_semaphore()
    for k in range(1, 8):
        pl.semaphore_signal(barrier, inc=1, device_id=yc_peer(k)[1], device_id_type=MESH)
        pl.semaphore_signal(barrier, inc=1, device_id=z_peer(k)[1], device_id_type=MESH)
    for k in range(1, 4):
        pl.semaphore_signal(barrier, inc=1, device_id=(sp, lax.rem(x + k, 4)), device_id_type=MESH)

    loads = [
        pltpu.make_async_copy(project_hbm, project, w_sem.at[0]),
        pltpu.make_async_copy(gate_hbm, w_gate, w_sem.at[1]),
        pltpu.make_async_copy(linear_hbm, w_linear, w_sem.at[2]),
        pltpu.make_async_copy(down_hbm, w_down, w_sem.at[3]),
    ]
    for load in loads:
        load.start()

    r_id, t_id = iota((192, 192), 0), iota((192, 192), 1)
    order = (t_id == lax.rem(r_id, 8) * SEGMENT + r_id // 8).astype(F32).astype(BF16)
    order_back = (r_id == lax.rem(t_id, 8) * SEGMENT + t_id // 8).astype(F32).astype(BF16)
    inputs = dot(order, mixer_input[...])
    inputs_bf = inputs.astype(BF16)
    double = jnp.concatenate([inputs_bf, inputs_bf], axis=1)

    gate_rows = jnp.exp(log_gate[...])
    g1 = gate_rows.astype(BF16).astype(F32)
    g2 = (gate_rows - g1).astype(BF16).astype(F32)
    g3 = gate_rows - g1 - g2
    three = jnp.concatenate([g1, g2, g3], axis=0).astype(BF16)
    three = dot_nt(three, order).astype(BF16)
    widen = (lax.rem(iota((24, 512), 0), 8) == iota((24, 512), 1) // 64).astype(F32).astype(BF16)
    wide = dot_tn(three, widen)
    for q in range(4):
        gates[q] = wide[:, 128 * q : 128 * (q + 1)]

    step, power24, power192, power1536 = [], [], [], []
    scale = []
    for d in range(2):
        rate, turn = decay_rate[d], turn_rate[d]
        retain = jnp.exp(-rate)
        step.append((expand(retain * jnp.cos(turn)), expand(retain * jnp.sin(turn))))
        scale.append(expand(jnp.sqrt(one_minus_exp_neg(2.0 * rate))))
        p = step[d]
        for _ in range(3):
            p = cmul(p, p)
        p24 = cmul(cmul(p, p), p)
        power24.append(p24)
        p = p24
        for _ in range(3):
            p = cmul(p, p)
        power192.append(p)
        for _ in range(3):
            p = cmul(p, p)
        power1536.append(p)

    def block_diagonal(table, q):
        both = jnp.concatenate([table, table], axis=1)
        group = iota((128, 128), 0) // 16
        lane = iota((128, 128), 1)
        return jnp.where(group == 2 * q + (lane >= 64).astype(jnp.int32), both, 0.0)

    for d in range(2):
        for part, table_ref in enumerate((drive_real, drive_imag)):
            table = table_ref[pl.ds(128 * d, 128), :]
            for q in range(0, 4, 2):
                cols = jnp.concatenate([block_diagonal(table, q), block_diagonal(table, q + 1)], axis=1)
                high, low = halves(cols * scale[d][:, 128 * q : 128 * (q + 2)])
                pushed = dot(double, jnp.concatenate([high, low], axis=0))
                push[2 * d + part, q] = pushed[:, :128]
                push[2 * d + part, q + 1] = pushed[:, 128:]

    steps = [
        [
            tuple(jnp.broadcast_to(step[d][m][:, 128 * q : 128 * (q + 1)], (8, 128)) for m in range(2))
            for q in range(4)
        ]
        for d in range(2)
    ]

    def sweep(initial, final):
        def body(j, carried):
            states, decay = carried
            new = []
            new_decay = []
            for d in range(2):
                at = pl.multiple_of((j if d == 0 else SEGMENT - 1 - j) * 8, 8)
                for q in range(4):
                    re, im = states[2 * (4 * d + q)], states[2 * (4 * d + q) + 1]
                    g = gates[q, pl.ds(at, 8), :]
                    if d == 0 and not final:
                        new_decay.append(decay[q] * g)
                    sr, si = steps[d][q]
                    nr = g * (sr * re - si * im) + push[2 * d, q, pl.ds(at, 8), :]
                    ni = g * (sr * im + si * re) + push[2 * d + 1, q, pl.ds(at, 8), :]
                    if final:
                        push[2 * d, q, pl.ds(at, 8), :] = nr
                        push[2 * d + 1, q, pl.ds(at, 8), :] = ni
                    new += [nr, ni]
            return tuple(new), tuple(new_decay)

        ones = () if final else tuple(jnp.ones((8, 128), F32) for _ in range(4))
        return lax.fori_loop(0, SEGMENT, body, (initial, ones))

    zeros = tuple(jnp.zeros((8, 128), F32) for _ in range(16))
    ends, decay = sweep(zeros, False)
    decay = jnp.concatenate(decay, axis=1)
    enter = []
    for d in range(2):
        s = tuple(jnp.concatenate([ends[2 * (4 * d + q) + m] for q in range(4)], axis=1) for m in range(2))
        a = tuple(decay * p for p in power24[d])
        a, s = inclusive(a, s, d == 1)
        enter.append(exclusive(a, s, d == 1))
        last = 0 if d == 1 else 7
        for m in range(2):
            msg1[pl.ds(2 * d + m, 1), :] = s[m][last : last + 1, :]
    total_decay = product(decay)
    msg1[pl.ds(4, 4), :] = total_decay[0:4, :]

    pl.semaphore_wait(barrier, 17)

    def level(msg, recv, peer, me, index, powers):
        for k in range(1, 8):
            send(msg, recv.at[me], small_send.at[index], small_recv.at[index], peer(k)[1])
        recv[pl.ds(me, 1)] = msg[...][None]
        settle(recv.at[pl.ds(0, 7)], small_recv.at[index])
        decays = recv[:, 4, :]
        found = []
        for d in range(2):
            s = tuple(recv[:, 2 * d + m, :] for m in range(2))
            a = tuple(decays * p for p in powers[d])
            a, s = inclusive(a, s, d == 1)
            ea, es = exclusive(a, s, d == 1)
            last = 0 if d == 1 else 7
            found.append(
                (
                    tuple(pick(v, me) for v in ea),
                    tuple(pick(v, me) for v in es),
                    tuple(v[last : last + 1, :] for v in s),
                )
            )
        return found, product(decays)

    found1, plane_decay = level(msg1, recv1, yc_peer, yc, 0, power192)
    for d in range(2):
        for m in range(2):
            msg2[pl.ds(2 * d + m, 1), :] = found1[d][2][m]
    msg2[pl.ds(4, 4), :] = plane_decay[0:4, :]
    found2, _ = level(msg2, recv2, z_peer, z, 1, power1536)
    initial = []
    for d in range(2):
        pa, ps, _ = found1[d]
        carry = cmul(pa, found2[d][1])
        carry = tuple(c + p for c, p in zip(carry, ps))
        ea, es = enter[d]
        first = cmul(ea, carry)
        first = tuple(f + e for f, e in zip(first, es))
        for q in range(4):
            initial += [f[:, 128 * q : 128 * (q + 1)] for f in first]
    sweep(tuple(initial), True)

    readout = None
    for index in range(4):
        d, part = divmod(index, 2)
        table = (read_real, read_imag)[part][pl.ds(128 * d, 128), :]
        table = table if part == 0 else -table
        for q in range(0, 4, 2):
            s_high, s_low = halves(jnp.concatenate([push[index, q], push[index, q + 1]], axis=1))
            cols = jnp.concatenate([block_diagonal(table, q), block_diagonal(table, q + 1)], axis=1)
            r_high, r_low = halves(cols)
            term = dot_nt(s_high, r_high) + dot_nt(s_low, r_high) + dot_nt(s_high, r_low)
            readout = term if readout is None else readout + term
    readout = readout + skip_gain[...] * inputs
    inner = 0.7978845608028654 * (readout + 0.044715 * readout * readout * readout)
    activated = (0.5 * readout * (1.0 + jnp.tanh(inner))).astype(BF16)
    activated = dot(order_back, activated).astype(BF16)
    act_out[...] = activated.reshape(4, 48, 128)
    for k in range(1, 4):
        other = lax.rem(x + k, 4)
        send(act_out.at[other], act_in.at[x], small_send.at[2], small_recv.at[2], (sp, other))
    act_in[pl.ds(x, 1)] = act_out[pl.ds(x, 1)]

    chosen = routes[...].astype(F32)
    weights = expert_weight[...]
    mixing = group_weight[...] * weights / jnp.sum(weights, axis=0, keepdims=True)
    own = iota((192, 128), 0) == 48 * x + iota((192, 128), 1)
    own = (own & (iota((192, 128), 1) < 48)).astype(F32)
    chosen = jnp.dot(chosen, own, precision=lax.Precision.HIGHEST, preferred_element_type=F32)
    mixing = jnp.dot(mixing, own, precision=lax.Precision.HIGHEST, preferred_element_type=F32)
    slot, lane = iota((128, 128), 0), iota((128, 128), 1)
    expert = (lax.rem(slot, 16) // 2 * 8 + slot // 16).astype(F32)
    first = (chosen[0:1, :] == expert) & (lane < 48)
    second = (chosen[1:2, :] == expert) & (lane < 48)
    match = jnp.where(first | second, 1.0, 0.0)
    earlier = (slot < lane).astype(F32).astype(BF16)
    rank = dot(match.astype(BF16), earlier)
    taken = jnp.where(rank == lax.rem(slot, 2).astype(F32), match, 0.0)
    combine = taken * jnp.where(first, mixing[0:1, :], mixing[1:2, :])
    combine_high, combine_low = halves(combine.T)
    taken = taken.astype(BF16)
    r_id, c_id = slot, lane
    swapped = lax.rem(r_id, 16) // 2 * 16 + r_id // 16 * 2 + lax.rem(r_id, 2)
    swap = (c_id == swapped).astype(F32).astype(BF16)

    rows[pl.ds(48, 80), :] = jnp.zeros((80, CHUNKS * WIDE), BF16)
    loads[0].wait()
    settle(act_in.at[pl.ds(0, 3)], small_recv.at[2])
    channels = jnp.concatenate([act_in[m] for m in range(4)], axis=1)
    total = jnp.zeros((48, 1), F32)
    for c in range(CHUNKS):
        cols = pl.ds(WIDE * c, WIDE)
        v = deep_alpha * residual[:, cols].astype(F32) + dot(channels, project[:, cols])
        middle[:, cols] = v
        total = total + jnp.sum(v, axis=1, keepdims=True)
    mean = total / (CHUNKS * WIDE)
    total = jnp.zeros((48, 1), F32)
    for c in range(CHUNKS):
        center = middle[:, pl.ds(WIDE * c, WIDE)] - mean
        total = total + jnp.sum(center * center, axis=1, keepdims=True)
    factor = lax.rsqrt(total / (CHUNKS * WIDE) + norm_epsilon)
    for c in range(CHUNKS):
        cols = pl.ds(WIDE * c, WIDE)
        v = (middle[:, cols] - mean) * factor * norm_gain[:, cols]
        middle[:, cols] = v
        rows[pl.ds(0, 48), cols] = v.astype(BF16)
        out1[:, :, cols] = dot(taken, rows[:, cols]).astype(BF16).reshape(8, 16, WIDE)
        for k in range(1, 8):
            other, device = yc_peer(k)
            send(out1.at[other, :, cols], in1.at[yc, :, cols], yc_send.at[0], yc_recv.at[0, c], device)
        in1[pl.ds(yc, 1), :, cols] = out1[pl.ds(yc, 1), :, cols]

    for c in range(CHUNKS):
        cols = pl.ds(WIDE * c, WIDE)
        settle(in1.at[pl.ds(0, 7), :, cols], yc_recv.at[0, c])
        moved = dot(swap, in1[:, :, cols].reshape(128, WIDE)).astype(BF16)
        out2[:, :, cols] = moved.reshape(8, 16, WIDE)
        for k in range(1, 8):
            other, device = z_peer(k)
            send(out2.at[other, :, cols], xin.at[0, z, :, cols], z_send.at[0], z_recv.at[0, c], device)
        xin[0, pl.ds(z, 1), :, cols] = out2[pl.ds(z, 1), :, cols]

    low, high = pl.ds(0, 4), pl.ds(4, 4)

    def spread(c):
        cols = pl.ds(WIDE * c, WIDE)
        settle(xin.at[0, pl.ds(0, 7), :, cols], z_recv.at[0, c])
        send(xin.at[0, :, :, cols], xin.at[1, :, :, cols], x_send.at[0], x_recv.at[0, c], (sp, right))
        send(xin.at[0, :, :, cols], xin.at[2, :, :, cols], x_send.at[1], x_recv.at[1, c], (sp, left))

    def pass_on(c):
        cols = pl.ds(WIDE * c, WIDE)
        settle(xin.at[1, :, :, cols], x_recv.at[0, c])
        send(xin.at[1, low, :, cols], xin.at[3, low, :, cols], x_send.at[2], o_recv.at[0, c], (sp, right))
        settle(xin.at[2, :, :, cols], x_recv.at[1, c])
        send(xin.at[2, high, :, cols], xin.at[3, high, :, cols], x_send.at[3], o_recv.at[1, c], (sp, left))

    def multiply(c):
        cols = pl.ds(WIDE * c, WIDE)
        settle(xin.at[3, low, :, cols], o_recv.at[0, c])
        settle(xin.at[3, high, :, cols], o_recv.at[1, c])
        block = xin[:, :, :, cols].reshape(512, WIDE)
        for acc, weight in ((gate_acc, w_gate), (linear_acc, w_linear)):
            term = dot(block, weight[cols, :])
            acc[...] = term if c == 0 else acc[...] + term

    loads[1].wait()
    loads[2].wait()
    for c in range(CHUNKS + 2):
        if c < CHUNKS:
            spread(c)
        if 1 <= c <= CHUNKS:
            pass_on(c - 1)
        if c >= 2:
            multiply(c - 2)
    gate = gate_acc[...]
    hidden[...] = (gate / (1.0 + jnp.exp(-gate)) * linear_acc[...]).astype(BF16)
    loads[3].wait()

    def partial(source, c):
        part = dot(hidden[pl.ds(128 * source, 128), :], w_down[:, pl.ds(WIDE * c, WIDE)])
        return part.reshape(8, 16, WIDE)

    def start_sums(c):
        cols = pl.ds(WIDE * c, WIDE)
        opp_out[:, :, cols] = partial(3, c).astype(BF16)
        send(opp_out.at[low, :, cols], fwd_r.at[:, :, cols], rs_send.at[0], rs_recv.at[0, c], (sp, right))
        send(opp_out.at[high, :, cols], fwd_l.at[:, :, cols], rs_send.at[1], rs_recv.at[1, c], (sp, left))
        part = partial(2, c)
        right_out[high, :, cols] = part[4:8].astype(BF16)
        keep_r[:, :, cols] = part[0:4]
        send(right_out.at[high, :, cols], from_l.at[high, :, cols], rs_send.at[2], rs_recv.at[2, c], (sp, right))
        part = partial(1, c)
        left_out[low, :, cols] = part[0:4].astype(BF16)
        keep_l[:, :, cols] = part[4:8]
        send(left_out.at[low, :, cols], from_r.at[low, :, cols], rs_send.at[3], rs_recv.at[3, c], (sp, left))

    def add_on(c):
        cols = pl.ds(WIDE * c, WIDE)
        settle(fwd_r.at[:, :, cols], rs_recv.at[0, c])
        right_out[low, :, cols] = (keep_r[:, :, cols] + fwd_r[:, :, cols].astype(F32)).astype(BF16)
        send(right_out.at[low, :, cols], from_l.at[low, :, cols], rs_send.at[4], rs_recv.at[4, c], (sp, right))
        settle(fwd_l.at[:, :, cols], rs_recv.at[1, c])
        left_out[high, :, cols] = (keep_l[:, :, cols] + fwd_l[:, :, cols].astype(F32)).astype(BF16)
        send(left_out.at[high, :, cols], from_r.at[high, :, cols], rs_send.at[5], rs_recv.at[5, c], (sp, left))

    def finish_sums(c):
        cols = pl.ds(WIDE * c, WIDE)
        part = partial(0, c)
        settle(from_l.at[high, :, cols], rs_recv.at[2, c])
        settle(from_r.at[low, :, cols], rs_recv.at[3, c])
        settle(from_l.at[low, :, cols], rs_recv.at[4, c])
        settle(from_r.at[high, :, cols], rs_recv.at[5, c])
        part = part + from_l[:, :, cols].astype(F32) + from_r[:, :, cols].astype(F32)
        ans[:, :, cols] = part.astype(BF16)
        for k in range(1, 8):
            other, device = z_peer(k)
            send(ans.at[other, :, cols], b2in.at[z, :, cols], z_send.at[1], z_recv.at[1, c], device)
        b2in[pl.ds(z, 1), :, cols] = ans[pl.ds(z, 1), :, cols]

    def go_home(c):
        cols = pl.ds(WIDE * c, WIDE)
        settle(b2in.at[pl.ds(0, 7), :, cols], z_recv.at[1, c])
        moved = dot(swap, b2in[:, :, cols].reshape(128, WIDE)).astype(BF16)
        b2out[:, :, cols] = moved.reshape(8, 16, WIDE)
        for k in range(1, 8):
            other, device = yc_peer(k)
            send(b2out.at[other, :, cols], b1in.at[yc, :, cols], yc_send.at[1], yc_recv.at[1, c], device)
        b1in[pl.ds(yc, 1), :, cols] = b2out[pl.ds(yc, 1), :, cols]

    for c in range(CHUNKS + 3):
        if c < CHUNKS:
            start_sums(c)
        if 1 <= c <= CHUNKS:
            add_on(c - 1)
        if 2 <= c <= CHUNKS + 1:
            finish_sums(c - 2)
        if c >= 3:
            go_home(c - 3)

    total = jnp.zeros((48, 1), F32)
    for c in range(CHUNKS):
        cols = pl.ds(WIDE * c, WIDE)
        settle(b1in.at[pl.ds(0, 7), :, cols], yc_recv.at[1, c])
        back = b1in[:, :, cols].reshape(128, WIDE)
        routed = dot(combine_high, back) + dot(combine_low, back)
        v = deep_alpha * middle[:, cols] + routed[0:48, :]
        middle[:, cols] = v
        total = total + jnp.sum(v, axis=1, keepdims=True)
    mean = total / (CHUNKS * WIDE)
    total = jnp.zeros((48, 1), F32)
    for c in range(CHUNKS):
        center = middle[:, pl.ds(WIDE * c, WIDE)] - mean
        total = total + jnp.sum(center * center, axis=1, keepdims=True)
    factor = lax.rsqrt(total / (CHUNKS * WIDE) + norm_epsilon)
    for c in range(CHUNKS):
        cols = pl.ds(WIDE * c, WIDE)
        out[:, cols] = ((middle[:, cols] - mean) * factor * final_gain[:, cols]).astype(BF16)

    for index, recv in enumerate((recv1, recv2)):
        settle(recv.at[pl.ds(0, 7)], small_send.at[index])
    settle(act_in.at[pl.ds(0, 3)], small_send.at[2])
    for index in range(2):
        settle(out1.at[pl.ds(0, 7)], yc_send.at[index])
        settle(out2.at[pl.ds(0, 7)], z_send.at[index])
        settle(xin.at[0], x_send.at[index])
        settle(xin.at[0, low], x_send.at[2 + index])
    for index in range(6):
        settle(fwd_r, rs_send.at[index])


def on_device(
    residual, mixer_input, log_gate, decay_rate, turn_rate, drive_real, drive_imaginary, read_real,
    read_imaginary, skip_gain, project_weight, norm_gain, final_gain, routes, group_weight,
    expert_weight, gate_weight, linear_weight, down_weight,
):
    vmem = pl.BlockSpec(memory_space=pltpu.VMEM)
    hbm = pl.BlockSpec(memory_space=pl.ANY)
    dma = pltpu.SemaphoreType.DMA
    slab = pltpu.VMEM((8, 16, 2048), BF16)
    half = pltpu.VMEM((4, 16, 2048), BF16)
    return pl.pallas_call(
        kernel,
        out_shape=jax.ShapeDtypeStruct((48, 2048), BF16),
        in_specs=[vmem] * 10 + [hbm] + [vmem] * 5 + [hbm] * 3,
        out_specs=vmem,
        scratch_shapes=[
            pltpu.VMEM((512, 2048), BF16),
            pltpu.VMEM((2048, 256), BF16),
            pltpu.VMEM((2048, 256), BF16),
            pltpu.VMEM((256, 2048), BF16),
            pltpu.VMEM((4, 192, 128), F32),
            pltpu.VMEM((4, 4, 192, 128), F32),
            pltpu.VMEM((8, 512), F32),
            pltpu.VMEM((8, 8, 512), F32),
            pltpu.VMEM((8, 512), F32),
            pltpu.VMEM((8, 8, 512), F32),
            pltpu.VMEM((4, 48, 128), BF16),
            pltpu.VMEM((4, 48, 128), BF16),
            pltpu.VMEM((48, 2048), F32),
            pltpu.VMEM((128, 2048), BF16),
            slab, slab, slab,
            pltpu.VMEM((4, 8, 16, 2048), BF16),
            pltpu.VMEM((512, 256), F32),
            pltpu.VMEM((512, 256), F32),
            pltpu.VMEM((512, 256), BF16),
            slab, half, half,
            slab, slab, slab, slab,
            pltpu.VMEM((4, 16, 2048), F32),
            pltpu.VMEM((4, 16, 2048), F32),
            slab, slab, slab, slab,
            dma((4,)), dma((3,)), dma((3,)),
            dma((2,)), dma((2, CHUNKS)), dma((2,)), dma((2, CHUNKS)),
            dma((4,)), dma((2, CHUNKS)), dma((2, CHUNKS)),
            dma((6,)), dma((6, CHUNKS)),
        ],
        compiler_params=pltpu.CompilerParams(
            collective_id=0, has_side_effects=True, vmem_limit_bytes=60 * 1024 * 1024
        ),
        name="layer",
    )(
        residual, mixer_input, log_gate.T, decay_rate, turn_rate,
        drive_real.reshape(256, 64), drive_imaginary.reshape(256, 64),
        read_real.reshape(256, 64), read_imaginary.reshape(256, 64),
        skip_gain.reshape(1, 128), project_weight, norm_gain.reshape(1, 2048),
        final_gain.reshape(1, 2048), routes.T, group_weight.reshape(1, 192), expert_weight.T,
        gate_weight[0], linear_weight[0], down_weight[0],
    )


def solution(mesh):
    placed = (
        P(("sp", "tp"), None),
        P("sp", "tp"),
        P("sp", "tp"),
        P(None, "tp", None),
        P(None, "tp", None),
        P(None, "tp", None, None),
        P(None, "tp", None, None),
        P(None, "tp", None, None),
        P(None, "tp", None, None),
        P("tp"),
        P(),
        P(),
        P(),
        P("sp", None),
        P("sp"),
        P("sp", None),
        P("sp", None, "tp"),
        P("sp", None, "tp"),
        P("sp", "tp", None),
    )
    return jax.shard_map(
        on_device, mesh=mesh, in_specs=placed, out_specs=P(("sp", "tp"), None), check_vma=False
    )
```

profile of v0, /device:TPU:1, one launch (start us, length us, event | category | flops | bytes accessed | tf_op | source)
XLA Modules:
  0.0 95.3 jit_solution(10930997819923896453)
XLA Ops:
  0.0 93.7 %layer.1 = bf16[48,2048]{1,0:T(8,128)(2,1)} custom-call(bf16[48,2048]{1,0:T(8,128)(2,1)} %residual.1, bf16[192,128]{1,0:T(8,128)(2,1)} %mixer_input.1, f32[8,192]{1,0:T(8,128)} %bitcast.21, f32[2,8,64]{2,1,0:T(8,128)} %decay_rate.1, f32[2,8,64]{2,1,0:T(8,128)} %turn_rate.1, f32[256,64]{1,0:T(8,128)} %bitcast.17, f32[256,64]{1,0:T(8,128)} %bitcast.18, ...), custom_call_target="tpu_custom_call" | custom-call | tf_op jit(solution)/shard_map/layer/pallas_call | solution.py:504
  93.7 1.6 %copy.21 = bf16[48,2048]{1,0:T(8,128)(2,1)} copy(bf16[48,2048]{1,0:T(8,128)(2,1)} %layer.1) | data formatting | bytes 393216
where the time goes:
time: 95.5 us; the launch traced here: 95.3 us
  Pallas kernels  93.7 us (98%)
  local copies, waits for them, and re-layouts  1.62 us (2%)
    pallas_call x1, Pallas kernels, on_device(): pl.pallas_call(kernel, out_shape=jax.ShapeDtypeStruct((48, 2048), BF16),...  93.7 us

commit v1 on v0

v1 whole, which is shorter than its diff:
```python
import jax
import jax.numpy as jnp
from jax import lax
from jax.experimental import pallas as pl
from jax.experimental.pallas import tpu as pltpu
from jax.sharding import PartitionSpec as P

MESH = pl.DeviceIdType.MESH
F32 = jnp.float32
BF16 = jnp.bfloat16
deep_alpha = 2.0**0.25
norm_epsilon = 1e-05
SEGMENT = 24
CHUNKS = 4
WIDE = 512
HALF = 1024
ORDER = (0, 1, 7, 2, 6, 3, 5, 4)
LANDS = tuple(ORDER.index((8 - k) % 8) for k in ORDER)


def iota(shape, dim):
    return lax.broadcasted_iota(jnp.int32, shape, dim)


def cmul(a, b):
    return (a[0] * b[0] - a[1] * b[1], a[0] * b[1] + a[1] * b[0])


def dot(a, b):
    return jnp.dot(a, b, preferred_element_type=F32)


def dot_nt(a, b):
    return lax.dot_general(a, b, (((1,), (1,)), ((), ())), preferred_element_type=F32)


def dot_tn(a, b):
    return lax.dot_general(a, b, (((0,), (0,)), ((), ())), preferred_element_type=F32)


def halves(value):
    high = value.astype(BF16)
    return high, (value - high.astype(F32)).astype(BF16)


def one_minus_exp_neg(x):
    series = x * (1.0 - x * (0.5 - x * (1.0 / 6 - x * (1.0 / 24 - x * (1.0 / 120 - x / 720)))))
    return jnp.where(x < 0.25, series, 1.0 - jnp.exp(-x))


def expand(value):
    both = jnp.concatenate([value, value], axis=1)
    row, lane = iota((8, 128), 0), iota((8, 128), 1)
    parts = [
        jnp.sum(jnp.where(row == 2 * q + (lane >= 64).astype(jnp.int32), both, 0.0), axis=0, keepdims=True)
        for q in range(4)
    ]
    return jnp.concatenate(parts, axis=1)


def inclusive(a, s, backward):
    row = iota(s[0].shape, 0)
    for shift in (1, 2, 4):
        ok = row < 8 - shift if backward else row >= shift
        turn = 8 - shift if backward else shift
        pa = tuple(pltpu.roll(v, turn, 0) for v in a)
        ps = tuple(pltpu.roll(v, turn, 0) for v in s)
        na, ns = cmul(a, pa), cmul(a, ps)
        s = tuple(jnp.where(ok, n + o, o) for n, o in zip(ns, s))
        a = tuple(jnp.where(ok, n, o) for n, o in zip(na, a))
    return a, s


def exclusive(a, s, backward):
    row = iota(s[0].shape, 0)
    ok = row < 7 if backward else row >= 1
    turn = 7 if backward else 1
    ident = (1.0, 0.0)
    ea = tuple(jnp.where(ok, pltpu.roll(v, turn, 0), i) for v, i in zip(a, ident))
    es = tuple(jnp.where(ok, pltpu.roll(v, turn, 0), 0.0) for v in s)
    return ea, es


def product(g):
    for shift in (1, 2, 4):
        g = g * pltpu.roll(g, shift, 0)
    return g


def pick(value, index):
    row = iota(value.shape, 0)
    return jnp.sum(jnp.where(row == index, value, 0.0), axis=0, keepdims=True)


INPUTS = (
    ((48, 2048), BF16), ((192, 128), BF16), ((8, 192), F32), ((2, 8, 64), F32), ((2, 8, 64), F32),
    ((256, 64), F32), ((256, 64), F32), ((256, 64), F32), ((256, 64), F32), ((1, 128), F32),
    ((512, 2048), BF16), ((1, 2048), F32), ((2, 192), jnp.int32), ((1, 192), F32), ((2, 192), F32),
    ((2048, 256), BF16), ((2048, 256), BF16), ((256, 2048), BF16),
)


def kernel(*refs):
    count = len(INPUTS)
    sources, out, held = refs[:count], refs[count], refs[count + 1 : 2 * count + 1]
    (
        residual, mixer_input, log_gate, decay_rate, turn_rate, drive_real, drive_imag, read_real,
        read_imag, skip_gain, project, norm_gain, routes, group_weight, expert_weight,
        w_gate, w_linear, w_down,
    ) = held
    (
        gates, push, msg1, recv1, msg2, recv2, act_out, act_in, middle, rows, tables, taken, combine,
        swap, out1, in1, out2, xin, hidden, opp_out, fwd_r, fwd_l, right_out, left_out, from_l,
        from_r, keep_r, keep_l, keep_o, ans, b2in, b2out, b1in,
        w_sem, small_send, small_recv, yc_send, yc_recv, z_send, z_recv, z_back, x_send, x_recv,
        o_recv, rs_send, rs_recv,
    ) = refs[2 * count + 1 :]
    sp, x = lax.axis_index("sp"), lax.axis_index("tp")
    z, yc = sp // 8, lax.rem(sp, 8)
    right, left = lax.rem(x + 1, 4), lax.rem(x + 3, 4)

    def yc_peer(k):
        other = lax.rem(yc + k, 8)
        return other, (z * 8 + other, x)

    def z_peer(k):
        other = lax.rem(z + k, 8)
        return other, (other * 8 + yc, x)

    def send(src, dst, s_sem, r_sem, device):
        pltpu.make_async_remote_copy(
            src_ref=src, dst_ref=dst, send_sem=s_sem, recv_sem=r_sem,
            device_id=device, device_id_type=MESH,
        ).start()

    def settle(ref, sem):
        pltpu.make_async_copy(ref, ref, sem).wait()

    barrier = pltpu.get_barrier_semaphore()
    for k in (4, 3, 5, 2, 6, 1, 7):
        pl.semaphore_signal(barrier, inc=1, device_id=z_peer(k)[1], device_id_type=MESH)
    for k in range(1, 8):
        pl.semaphore_signal(barrier, inc=1, device_id=yc_peer(k)[1], device_id_type=MESH)
    for k in range(1, 4):
        pl.semaphore_signal(barrier, inc=1, device_id=(sp, lax.rem(x + k, 4)), device_id_type=MESH)
    loads = [pltpu.make_async_copy(a, b, w_sem.at[n]) for n, (a, b) in enumerate(zip(sources, held))]
    first_needed = (1, 2, 3, 4, 5, 6)
    for n in first_needed:
        loads[n].start()
    for n in range(count):
        if n not in first_needed:
            loads[n].start()
    for n in first_needed:
        loads[n].wait()

    r_id, t_id = iota((192, 192), 0), iota((192, 192), 1)
    order = (t_id == lax.rem(r_id, 8) * SEGMENT + r_id // 8).astype(F32).astype(BF16)
    inputs_bf = dot(order, mixer_input[...]).astype(BF16)
    double = jnp.concatenate([inputs_bf, inputs_bf], axis=1)

    gate_rows = jnp.exp(log_gate[...])
    g1 = gate_rows.astype(BF16).astype(F32)
    g2 = (gate_rows - g1).astype(BF16).astype(F32)
    g3 = gate_rows - g1 - g2
    three = jnp.concatenate([g1, g2, g3], axis=0).astype(BF16)
    three = dot_nt(three, order).astype(BF16)
    widen = (lax.rem(iota((24, 512), 0), 8) == iota((24, 512), 1) // 64).astype(F32).astype(BF16)
    wide = dot_tn(three, widen)
    for q in range(4):
        gates[q] = wide[:, 128 * q : 128 * (q + 1)]

    step, power24, power192, power1536 = [], [], [], []
    scale = []
    for d in range(2):
        rate, turn = decay_rate[d], turn_rate[d]
        retain = jnp.exp(-rate)
        step.append((expand(retain * jnp.cos(turn)), expand(retain * jnp.sin(turn))))
        scale.append(expand(jnp.sqrt(one_minus_exp_neg(2.0 * rate))))
        p = step[d]
        for _ in range(3):
            p = cmul(p, p)
        p24 = cmul(cmul(p, p), p)
        power24.append(p24)
        p = p24
        for _ in range(3):
            p = cmul(p, p)
        power192.append(p)
        for _ in range(3):
            p = cmul(p, p)
        power1536.append(p)

    def block_diagonal(table, q):
        both = jnp.concatenate([table, table], axis=1)
        group = iota((128, 128), 0) // 16
        lane = iota((128, 128), 1)
        return jnp.where(group == 2 * q + (lane >= 64).astype(jnp.int32), both, 0.0)

    def pair(table, q):
        return jnp.concatenate([block_diagonal(table, q), block_diagonal(table, q + 1)], axis=1)

    for d in range(2):
        for part, table_ref in enumerate((drive_real, drive_imag)):
            table = table_ref[pl.ds(128 * d, 128), :]
            for q in range(0, 4, 2):
                high, low = halves(pair(table, q) * scale[d][:, 128 * q : 128 * (q + 2)])
                pushed = dot(double, jnp.concatenate([high, low], axis=0))
                push[2 * d + part, q] = pushed[:, :128]
                push[2 * d + part, q + 1] = pushed[:, 128:]

    steps = [
        [
            tuple(jnp.broadcast_to(step[d][m][:, 128 * q : 128 * (q + 1)], (8, 128)) for m in range(2))
            for q in range(4)
        ]
        for d in range(2)
    ]

    def sweep(initial, final):
        def body(j, carried):
            states, decay = carried
            new = []
            new_decay = []
            for d in range(2):
                at = pl.multiple_of((j if d == 0 else SEGMENT - 1 - j) * 8, 8)
                for q in range(4):
                    re, im = states[2 * (4 * d + q)], states[2 * (4 * d + q) + 1]
                    g = gates[q, pl.ds(at, 8), :]
                    if d == 0 and not final:
                        new_decay.append(decay[q] * g)
                    sr, si = steps[d][q]
                    nr = g * (sr * re - si * im) + push[2 * d, q, pl.ds(at, 8), :]
                    ni = g * (sr * im + si * re) + push[2 * d + 1, q, pl.ds(at, 8), :]
                    if final:
                        push[2 * d, q, pl.ds(at, 8), :] = nr
                        push[2 * d + 1, q, pl.ds(at, 8), :] = ni
                    new += [nr, ni]
            return tuple(new), tuple(new_decay)

        ones = () if final else tuple(jnp.ones((8, 128), F32) for _ in range(4))
        return lax.fori_loop(0, SEGMENT, body, (initial, ones))

    def put(msg, d, m, row):
        for q in range(4):
            msg[2 * d, pl.ds(4 * m + q, 1), :] = row[:, 128 * q : 128 * (q + 1)]

    def put_decay(msg, value):
        for q in range(4):
            msg[1, pl.ds(q, 1), :] = value[0:1, 128 * q : 128 * (q + 1)]
            msg[1, pl.ds(4 + q, 1), :] = value[0:1, 128 * q : 128 * (q + 1)]

    zeros = tuple(jnp.zeros((8, 128), F32) for _ in range(16))
    ends, decay = sweep(zeros, False)
    decay = jnp.concatenate(decay, axis=1)
    enter = []
    for d in range(2):
        s = tuple(jnp.concatenate([ends[2 * (4 * d + q) + m] for q in range(4)], axis=1) for m in range(2))
        a = tuple(decay * p for p in power24[d])
        a, s = inclusive(a, s, d == 1)
        enter.append(exclusive(a, s, d == 1))
        last = 0 if d == 1 else 7
        for m in range(2):
            put(msg1, d, m, s[m][last : last + 1, :])
    put_decay(msg1, product(decay))

    pl.semaphore_wait(barrier, 17)

    def gathered(recv, slab, first_row):
        return jnp.concatenate([recv[:, slab, first_row + q, :] for q in range(4)], axis=1)

    def combined(recv, me, powers, masked):
        decays = gathered(recv, 1, 0)
        row = iota((8, 512), 0)
        found = []
        for d in range(2):
            s = tuple(gathered(recv, 2 * d, 4 * m) for m in range(2))
            if masked:
                used = row > me if d == 1 else row < me
                s = tuple(jnp.where(used, v, 0.0) for v in s)
            a = tuple(decays * p for p in powers[d])
            a, s = inclusive(a, s, d == 1)
            ea, es = exclusive(a, s, d == 1)
            last = 0 if d == 1 else 7
            found.append(
                (
                    tuple(pick(v, me) for v in ea),
                    tuple(pick(v, me) for v in es),
                    tuple(v[last : last + 1, :] for v in s),
                )
            )
        return found, decays

    for k in range(1, 8):
        send(msg1, recv1.at[yc], small_send.at[0], small_recv.at[0], yc_peer(k)[1])
    recv1[pl.ds(yc, 1)] = msg1[...][None]

    for n in (7, 8, 12, 13, 14):
        loads[n].wait()
    for index in range(4):
        d, part = divmod(index, 2)
        table = (read_real, read_imag)[part][pl.ds(128 * d, 128), :]
        table = table if part == 0 else -table
        for q in range(0, 4, 2):
            tables[index, q // 2] = jnp.concatenate(halves(pair(table, q)), axis=0)
    chosen = routes[...].astype(F32)
    weights = expert_weight[...]
    mixing = group_weight[...] * weights / jnp.sum(weights, axis=0, keepdims=True)
    own = iota((192, 128), 0) == 48 * x + iota((192, 128), 1)
    own = (own & (iota((192, 128), 1) < 48)).astype(F32)
    chosen = jnp.dot(chosen, own, precision=lax.Precision.HIGHEST, preferred_element_type=F32)
    mixing = jnp.dot(mixing, own, precision=lax.Precision.HIGHEST, preferred_element_type=F32)
    slot, lane = iota((128, 128), 0), iota((128, 128), 1)
    place = lax.rem(slot, 16) // 2
    offset = jnp.zeros_like(place)
    for i in range(1, 8):
        offset = jnp.where(place == i, ORDER[i], offset)
    expert = (lax.rem(z + offset, 8) * 8 + slot // 16).astype(F32)
    first = (chosen[0:1, :] == expert) & (lane < 48)
    second = (chosen[1:2, :] == expert) & (lane < 48)
    match = jnp.where(first | second, 1.0, 0.0)
    earlier = (slot < lane).astype(F32).astype(BF16)
    rank = dot(match.astype(BF16), earlier)
    mine = jnp.where(rank == lax.rem(slot, 2).astype(F32), match, 0.0)
    taken[...] = mine.astype(BF16)
    mine = mine * jnp.where(first, mixing[0:1, :], mixing[1:2, :])
    combine[0], combine[1] = halves(mine.T)
    swapped = place * 16 + slot // 16 * 2 + lax.rem(slot, 2)
    swap[...] = (lane == swapped).astype(F32).astype(BF16)
    rows[pl.ds(48, 80), :] = jnp.zeros((80, CHUNKS * WIDE), BF16)

    settle(recv1.at[pl.ds(0, 7)], small_recv.at[0])
    found1, decays = combined(recv1, yc, power192, False)
    for d in range(2):
        for m in range(2):
            put(msg2, d, m, found1[d][2][m])
    put_decay(msg2, product(decays))
    for k in (4, 3, 5, 2, 6, 1, 7):
        other, device = z_peer(k)
        part = pl.ds(jnp.where(other > z, 0, 1), 2)
        send(msg2.at[part], recv2.at[z, part], small_send.at[1], small_recv.at[1], device)
    recv2[pl.ds(z, 1)] = msg2[...][None]
    settle(recv2.at[pl.ds(0, 7), pl.ds(0, 2)], small_recv.at[1])
    found2, _ = combined(recv2, z, power1536, True)
    initial = []
    for d in range(2):
        pa, ps, _ = found1[d]
        carry = cmul(pa, found2[d][1])
        carry = tuple(c + p for c, p in zip(carry, ps))
        ea, es = enter[d]
        begin = cmul(ea, carry)
        begin = tuple(f + e for f, e in zip(begin, es))
        for q in range(4):
            initial += [f[:, 128 * q : 128 * (q + 1)] for f in begin]
    sweep(tuple(initial), True)

    loads[9].wait()
    readout = skip_gain[...] * inputs_bf.astype(F32)
    both = jnp.zeros((192, 256), F32)
    for index in range(4):
        for q in range(0, 4, 2):
            s_high, s_low = halves(jnp.concatenate([push[index, q], push[index, q + 1]], axis=1))
            both = both + dot_nt(s_high, tables[index, q // 2])
            readout = readout + dot_nt(s_low, tables[index, q // 2, pl.ds(0, 128), :])
    readout = readout + both[:, :128] + both[:, 128:]
    inner = 0.7978845608028654 * (readout + 0.044715 * readout * readout * readout)
    activated = (0.5 * readout * (1.0 + jnp.tanh(inner))).astype(BF16)
    r_id, t_id = iota((192, 192), 0), iota((192, 192), 1)
    order_back = (r_id == lax.rem(t_id, 8) * SEGMENT + t_id // 8).astype(F32).astype(BF16)
    activated = dot(order_back, activated).astype(BF16)
    act_out[...] = activated.reshape(4, 48, 128)
    for k in (2, 1, 3):
        other = lax.rem(x + k, 4)
        send(act_out.at[other], act_in.at[x], small_send.at[2], small_recv.at[2], (sp, other))
    act_in[pl.ds(x, 1)] = act_out[pl.ds(x, 1)]

    for n in (0, 10, 11):
        loads[n].wait()
    settle(act_in.at[pl.ds(0, 3)], small_recv.at[2])
    channels = jnp.concatenate([act_in[m] for m in range(4)], axis=1)
    total = jnp.zeros((48, 1), F32)
    for c in range(CHUNKS):
        cols = pl.ds(WIDE * c, WIDE)
        v = deep_alpha * residual[:, cols].astype(F32) + dot(channels, project[:, cols])
        middle[:, cols] = v
        total = total + jnp.sum(v, axis=1, keepdims=True)
    mean = total / (CHUNKS * WIDE)
    total = jnp.zeros((48, 1), F32)
    for c in range(CHUNKS):
        center = middle[:, pl.ds(WIDE * c, WIDE)] - mean
        total = total + jnp.sum(center * center, axis=1, keepdims=True)
    factor = lax.rsqrt(total / (CHUNKS * WIDE) + norm_epsilon)
    for c in range(CHUNKS):
        cols = pl.ds(WIDE * c, WIDE)
        v = (middle[:, cols] - mean) * factor * norm_gain[:, cols]
        middle[:, cols] = v
        rows[pl.ds(0, 48), cols] = v.astype(BF16)
        out1[:, :, cols] = dot(taken[...], rows[:, cols]).astype(BF16).reshape(8, 16, WIDE)
        for k in range(1, 8):
            other, device = yc_peer(k)
            send(out1.at[other, :, cols], in1.at[yc, :, cols], yc_send.at[0], yc_recv.at[0, c], device)
        in1[pl.ds(yc, 1), :, cols] = out1[pl.ds(yc, 1), :, cols]

    def side(h):
        return pl.ds(HALF * h, HALF)

    def start_z(i, h, cols):
        to = LANDS[i]
        send(
            out2.at[i, :, cols], xin.at[0, to, :, cols], z_send.at[0], z_recv.at[to, h],
            z_peer(ORDER[i])[1],
        )

    def spread(i, h, cols):
        block = xin.at[0, i, :, cols]
        rest = o_recv.at[i // 4]
        send(block, xin.at[1, i, :, cols], x_send.at[0], rest if h else x_recv.at[0, i], (sp, right))
        send(block, xin.at[2, i, :, cols], x_send.at[1], x_recv.at[1, i] if h else rest, (sp, left))

    def pass_on(i):
        block = xin.at[1, i, :, side(0)]
        settle(block, x_recv.at[0, i])
        send(block, xin.at[3, i, :, side(0)], x_send.at[2], o_recv.at[i // 4], (sp, right))
        block = xin.at[2, i, :, side(1)]
        settle(block, x_recv.at[1, i])
        send(block, xin.at[3, i, :, side(1)], x_send.at[3], o_recv.at[i // 4], (sp, left))

    for c in range(CHUNKS):
        cols = pl.ds(WIDE * c, WIDE)
        settle(in1.at[pl.ds(0, 7), :, cols], yc_recv.at[0, c])
        moved = dot(swap[...], in1[:, :, cols].reshape(128, WIDE)).astype(BF16)
        out2[:, :, cols] = moved.reshape(8, 16, WIDE)
        xin[0, 0, :, cols] = moved[0:16, :]
        for i in range(1, 4):
            start_z(i, c // 2, cols)
        spread(0, c // 2, cols)
    for i in range(4, 8):
        for h in range(2):
            start_z(i, h, side(h))

    def multiply(g):
        settle(xin.at[pl.ds(2, 2), pl.ds(4 * g, 4)], o_recv.at[g])
        block = xin[:, pl.ds(4 * g, 4)].reshape(256, 2048)
        gate = dot(block, w_gate[...])
        linear = dot(block, w_linear[...])
        hidden[g] = (gate / (1.0 + jnp.exp(-gate)) * linear).astype(BF16)

    low, high = pl.ds(0, 2), pl.ds(2, 2)

    def start_sums(g, c):
        cols = pl.ds(WIDE * c, WIDE)
        part = dot(hidden[g], w_down[:, cols]).reshape(4, 4, 16, WIDE)
        opp_out[g, :, :, cols] = part[3].astype(BF16)
        send(opp_out.at[g, low, :, cols], fwd_r.at[g, :, :, cols], rs_send.at[0], rs_recv.at[0, g, c], (sp, right))
        send(opp_out.at[g, high, :, cols], fwd_l.at[g, :, :, cols], rs_send.at[1], rs_recv.at[1, g, c], (sp, left))
        right_out[g, high, :, cols] = part[2, 2:4].astype(BF16)
        keep_r[g, :, :, cols] = part[2, 0:2]
        send(right_out.at[g, high, :, cols], from_l.at[g, high, :, cols], rs_send.at[2], rs_recv.at[2, g, c], (sp, right))
        left_out[g, low, :, cols] = part[1, 0:2].astype(BF16)
        keep_l[g, :, :, cols] = part[1, 2:4]
        send(left_out.at[g, low, :, cols], from_r.at[g, low, :, cols], rs_send.at[3], rs_recv.at[3, g, c], (sp, left))
        keep_o[g, :, :, cols] = part[0]

    def add_on(g, c):
        cols = pl.ds(WIDE * c, WIDE)
        settle(fwd_r.at[g, :, :, cols], rs_recv.at[0, g, c])
        right_out[g, low, :, cols] = (keep_r[g, :, :, cols] + fwd_r[g, :, :, cols].astype(F32)).astype(BF16)
        send(right_out.at[g, low, :, cols], from_l.at[g, low, :, cols], rs_send.at[2], rs_recv.at[2, g, c], (sp, right))
        settle(fwd_l.at[g, :, :, cols], rs_recv.at[1, g, c])
        left_out[g, high, :, cols] = (keep_l[g, :, :, cols] + fwd_l[g, :, :, cols].astype(F32)).astype(BF16)
        send(left_out.at[g, high, :, cols], from_r.at[g, high, :, cols], rs_send.at[3], rs_recv.at[3, g, c], (sp, left))

    def finish_sums(g, c):
        cols = pl.ds(WIDE * c, WIDE)
        settle(from_l.at[g, :, :, cols], rs_recv.at[2, g, c])
        settle(from_r.at[g, :, :, cols], rs_recv.at[3, g, c])
        part = keep_o[g, :, :, cols] + from_l[g, :, :, cols].astype(F32) + from_r[g, :, :, cols].astype(F32)
        ans[pl.ds(4 * g, 4), :, cols] = part.astype(BF16)
        for i in range(4 * g, 4 * g + 4):
            if i == 0:
                b2in[0, :, cols] = ans[0, :, cols]
                continue
            send(ans.at[i, :, cols], b2in.at[LANDS[i], :, cols], z_send.at[1], z_back.at[c], z_peer(ORDER[i])[1])

    def go_home(c):
        cols = pl.ds(WIDE * c, WIDE)
        settle(b2in.at[pl.ds(0, 7), :, cols], z_back.at[c])
        moved = dot(swap[...], b2in[:, :, cols].reshape(128, WIDE)).astype(BF16)
        b2out[:, :, cols] = moved.reshape(8, 16, WIDE)
        for k in range(1, 8):
            other, device = yc_peer(k)
            send(b2out.at[other, :, cols], b1in.at[yc, :, cols], yc_send.at[1], yc_recv.at[1, c], device)
        b1in[pl.ds(yc, 1), :, cols] = b2out[pl.ds(yc, 1), :, cols]

    for i in range(1, 8):
        for h in range(2):
            settle(xin.at[0, i, :, side(h)], z_recv.at[i, h])
            spread(i, h, side(h))
        pass_on(i - 1)
        if i == 1:
            for n in (15, 16, 17):
                loads[n].wait()
    multiply(0)
    pass_on(7)
    start_sums(0, 0)
    start_sums(0, 1)
    start_sums(0, 2)
    add_on(0, 0)
    multiply(1)
    start_sums(1, 0)
    start_sums(1, 1)
    add_on(0, 1)
    start_sums(1, 2)
    add_on(1, 0)
    start_sums(1, 3)
    add_on(1, 1)
    finish_sums(0, 0)
    finish_sums(0, 1)
    add_on(1, 2)
    finish_sums(1, 0)
    add_on(1, 3)
    start_sums(0, 3)
    finish_sums(1, 1)
    add_on(0, 2)
    finish_sums(1, 2)
    add_on(0, 3)
    finish_sums(1, 3)
    go_home(0)
    finish_sums(0, 2)
    finish_sums(0, 3)
    for c in range(1, CHUNKS):
        go_home(c)

    total = jnp.zeros((48, 1), F32)
    for c in range(CHUNKS):
        cols = pl.ds(WIDE * c, WIDE)
        settle(b1in.at[pl.ds(0, 7), :, cols], yc_recv.at[1, c])
        back = b1in[:, :, cols].reshape(128, WIDE)
        routed = dot(combine[0, pl.ds(0, 48), :], back) + dot(combine[1, pl.ds(0, 48), :], back)
        v = deep_alpha * middle[:, cols] + routed
        middle[:, cols] = v
        total = total + jnp.sum(v, axis=1, keepdims=True)
    mean = total / (CHUNKS * WIDE)
    total = jnp.zeros((48, 1), F32)
    for c in range(CHUNKS):
        center = middle[:, pl.ds(WIDE * c, WIDE)] - mean
        total = total + jnp.sum(center * center, axis=1, keepdims=True)
    factor = lax.rsqrt(total / (CHUNKS * WIDE) + norm_epsilon)
    for c in range(CHUNKS):
        cols = pl.ds(WIDE * c, WIDE)
        out[:, cols] = (middle[:, cols] - mean) * factor

    settle(recv1.at[pl.ds(0, 7)], small_send.at[0])
    settle(recv2.at[pl.ds(0, 7), pl.ds(0, 2)], small_send.at[1])
    settle(act_in.at[pl.ds(0, 3)], small_send.at[2])
    for index in range(2):
        settle(out1.at[pl.ds(0, 7)], yc_send.at[index])
        settle(out2.at[pl.ds(0, 7)], z_send.at[index])
        settle(xin.at[0], x_send.at[index])
        settle(xin.at[0, pl.ds(0, 4)], x_send.at[2 + index])
        settle(fwd_r, rs_send.at[index])
        settle(from_l, rs_send.at[2 + index])


def on_device(
    residual, mixer_input, log_gate, decay_rate, turn_rate, drive_real, drive_imaginary, read_real,
    read_imaginary, skip_gain, project_weight, norm_gain, final_gain, routes, group_weight,
    expert_weight, gate_weight, linear_weight, down_weight,
):
    dma = pltpu.SemaphoreType.DMA
    slab = pltpu.VMEM((8, 16, 2048), BF16)
    groups = pltpu.VMEM((2, 4, 16, 2048), BF16)
    half = pltpu.VMEM((2, 2, 16, 2048), BF16)
    normed = pl.pallas_call(
        kernel,
        out_shape=jax.ShapeDtypeStruct((48, 2048), F32),
        in_specs=[pl.BlockSpec(memory_space=pl.ANY)] * len(INPUTS),
        out_specs=pl.BlockSpec(memory_space=pltpu.VMEM),
        scratch_shapes=[pltpu.VMEM(shape, dtype) for shape, dtype in INPUTS]
        + [
            pltpu.VMEM((4, 192, 128), F32),
            pltpu.VMEM((4, 4, 192, 128), F32),
            pltpu.VMEM((3, 8, 128), F32),
            pltpu.VMEM((8, 3, 8, 128), F32),
            pltpu.VMEM((3, 8, 128), F32),
            pltpu.VMEM((8, 3, 8, 128), F32),
            pltpu.VMEM((4, 48, 128), BF16),
            pltpu.VMEM((4, 48, 128), BF16),
            pltpu.VMEM((48, 2048), F32),
            pltpu.VMEM((128, 2048), BF16),
            pltpu.VMEM((4, 2, 256, 256), BF16),
            pltpu.VMEM((128, 128), BF16),
            pltpu.VMEM((2, 128, 128), BF16),
            pltpu.VMEM((128, 128), BF16),
            slab, slab, slab,
            pltpu.VMEM((4, 8, 16, 2048), BF16),
            pltpu.VMEM((2, 256, 256), BF16),
            groups, half, half,
            groups, groups, groups, groups,
            pltpu.VMEM((2, 2, 16, 2048), F32),
            pltpu.VMEM((2, 2, 16, 2048), F32),
            pltpu.VMEM((2, 4, 16, 2048), F32),
            slab, slab, slab, slab,
            dma((len(INPUTS),)), dma((3,)), dma((3,)),
            dma((2,)), dma((2, CHUNKS)), dma((2,)), dma((8, 2)), dma((CHUNKS,)),
            dma((4,)), dma((2, 8)), dma((2,)),
            dma((4,)), dma((4, 2, CHUNKS)),
        ],
        compiler_params=pltpu.CompilerParams(
            collective_id=0, has_side_effects=True, vmem_limit_bytes=40 * 1024 * 1024
        ),
        name="layer",
    )(*(pltpu.with_memory_space_constraint(v, pltpu.HBM) for v in (
        residual, mixer_input, log_gate.T, decay_rate, turn_rate,
        drive_real.reshape(256, 64), drive_imaginary.reshape(256, 64),
        read_real.reshape(256, 64), read_imaginary.reshape(256, 64),
        skip_gain.reshape(1, 128), project_weight, norm_gain.reshape(1, 2048),
        routes.T, group_weight.reshape(1, 192), expert_weight.T,
        gate_weight[0], linear_weight[0], down_weight[0],
    )))
    return (normed * final_gain).astype(BF16)


def solution(mesh):
    placed = (
        P(("sp", "tp"), None),
        P("sp", "tp"),
        P("sp", "tp"),
        P(None, "tp", None),
        P(None, "tp", None),
        P(None, "tp", None, None),
        P(None, "tp", None, None),
        P(None, "tp", None, None),
        P(None, "tp", None, None),
        P("tp"),
        P(),
        P(),
        P(),
        P("sp", None),
        P("sp"),
        P("sp", None),
        P("sp", None, "tp"),
        P("sp", None, "tp"),
        P("sp", "tp", None),
    )
    return jax.shard_map(
        on_device, mesh=mesh, in_specs=placed, out_specs=P(("sp", "tp"), None), check_vma=False
    )
```

time: 95.5 us -> 83.4 us (0.87)
  Pallas kernels: 93.7 us -> 82.6 us
  local copies, waits for them, and re-layouts: 1.62 us -> 0.01 us
    pallas_call x1, Pallas kernels: 93.7 us -> 82.6 us  [on_device(): pl.pallas_call(kernel, out_shape=jax.ShapeDtypeStruct((48, 2048), F32), i...]
    unnamed x1 -> x2, local copies, waits for them, and re-layouts: 1.62 us -> 0.01 us
where the time goes in v1:
time: 83.4 us; the launch traced here: 83.3 us
  Pallas kernels  82.6 us (99%)
    pallas_call x1, Pallas kernels, on_device(): pl.pallas_call(kernel, out_shape=jax.ShapeDtypeStruct((48, 2048), F32), i...  82.6 us

profile of v1, /device:TPU:1, one launch (start us, length us, event | category | flops | bytes accessed | tf_op | source)
XLA Modules:
  0.0 83.3 jit_solution(10066726540128309993)
XLA Ops:
  0.0 0.0 copy-start
  0.0 82.6 %layer.1 = f32[48,2048]{1,0:T(8,128)S(1)} custom-call(bf16[48,2048]{1,0:T(8,128)(2,1)} %refs_0_.1, bf16[192,128]{1,0:T(8,128)(2,1)} %refs_1_.1, f32[8,192]{1,0:T(8,128)} %bitcast.20, f32[2,8,64]{2,1,0:T(8,128)} %refs_3_.1, f32[2,8,64]{2,1,0:T(8,128)} %refs_4_.1, f32[256,64]{1,0:T(8,128)} %bitcast.16, f32[256,64]{1,0:T(8,128)} %bitcast.17, ...), custom_call_target="tpu_custom_call" | custom-call | tf_op jit(solution)/shard_map/layer/pallas_call | solution.py:572
  82.6 0.0 copy-done
  82.6 0.7 multiply_convert_fusion
Async XLA Ops:
  0.0 82.6 %copy-start = (f32[2048]{0:T(1024)S(1)}, f32[2048]{0:T(1024)}, u32[]{:S(2)}) copy-start(f32[2048]{0:T(1024)} %param.31) | copy-start | bytes 24580

commit v2 on v1

--- a/solution.py
+++ b/solution.py
@@ -14,6 +14,7 @@
 CHUNKS = 4
 WIDE = 512
 HALF = 1024
+FAR = (4, 3, 5, 2, 6, 1, 7)
 ORDER = (0, 1, 7, 2, 6, 3, 5, 4)
 LANDS = tuple(ORDER.index((8 - k) % 8) for k in ORDER)
 
@@ -109,9 +110,8 @@
         w_gate, w_linear, w_down,
     ) = held
     (
-        gates, push, msg1, recv1, msg2, recv2, act_out, act_in, middle, rows, tables, taken, combine,
-        swap, out1, in1, out2, xin, hidden, opp_out, fwd_r, fwd_l, right_out, left_out, from_l,
-        from_r, keep_r, keep_l, keep_o, ans, b2in, b2out, b1in,
+        gates, push, msg1, recv1, msg2, recv2, dec1, keep1, dec2, keep2, act_out, act_in, middle, rows, tables, taken, combine,
+        swap, out1, in1, out2, xin, hidden, opp_out, fwd, right_out, left_out, sums, keep_r, keep_l, keep_o, ans, b2in, b2out, b1in,
         w_sem, small_send, small_recv, yc_send, yc_recv, z_send, z_recv, z_back, x_send, x_recv,
         o_recv, rs_send, rs_recv,
     ) = refs[2 * count + 1 :]
@@ -137,9 +137,9 @@
         pltpu.make_async_copy(ref, ref, sem).wait()
 
     barrier = pltpu.get_barrier_semaphore()
-    for k in (4, 3, 5, 2, 6, 1, 7):
+    for k in FAR:
         pl.semaphore_signal(barrier, inc=1, device_id=z_peer(k)[1], device_id_type=MESH)
-    for k in range(1, 8):
+    for k in FAR:
         pl.semaphore_signal(barrier, inc=1, device_id=yc_peer(k)[1], device_id_type=MESH)
     for k in range(1, 4):
         pl.semaphore_signal(barrier, inc=1, device_id=(sp, lax.rem(x + k, 4)), device_id_type=MESH)
@@ -241,12 +241,8 @@
 
     def put(msg, d, m, row):
         for q in range(4):
-            msg[2 * d, pl.ds(4 * m + q, 1), :] = row[:, 128 * q : 128 * (q + 1)]
-
-    def put_decay(msg, value):
-        for q in range(4):
-            msg[1, pl.ds(q, 1), :] = value[0:1, 128 * q : 128 * (q + 1)]
-            msg[1, pl.ds(4 + q, 1), :] = value[0:1, 128 * q : 128 * (q + 1)]
+            msg[d, pl.ds(4 * m + q, 1), :] = row[:, 128 * q : 128 * (q + 1)]
+
 
     zeros = tuple(jnp.zeros((8, 128), F32) for _ in range(16))
     ends, decay = sweep(zeros, False)
@@ -260,19 +256,19 @@
         last = 0 if d == 1 else 7
         for m in range(2):
             put(msg1, d, m, s[m][last : last + 1, :])
-    put_decay(msg1, product(decay))
+    dec1[0] = product(decay)[0:1, :]
 
     pl.semaphore_wait(barrier, 17)
 
     def gathered(recv, slab, first_row):
         return jnp.concatenate([recv[:, slab, first_row + q, :] for q in range(4)], axis=1)
 
-    def combined(recv, me, powers, masked):
-        decays = gathered(recv, 1, 0)
+    def combined(recv, kept, me, powers, masked):
+        decays = kept[:, 0, :]
         row = iota((8, 512), 0)
         found = []
         for d in range(2):
-            s = tuple(gathered(recv, 2 * d, 4 * m) for m in range(2))
+            s = tuple(gathered(recv, d, 4 * m) for m in range(2))
             if masked:
                 used = row > me if d == 1 else row < me
                 s = tuple(jnp.where(used, v, 0.0) for v in s)
@@ -289,9 +285,11 @@
             )
         return found, decays
 
-    for k in range(1, 8):
+    for k in FAR:
         send(msg1, recv1.at[yc], small_send.at[0], small_recv.at[0], yc_peer(k)[1])
+        send(dec1.at[0], keep1.at[yc], small_send.at[3], small_recv.at[3], yc_peer(k)[1])
     recv1[pl.ds(yc, 1)] = msg1[...][None]
+    keep1[pl.ds(yc, 1)] = dec1[...]
 
     for n in (7, 8, 12, 13, 14):
         loads[n].wait()
@@ -328,18 +326,22 @@
     rows[pl.ds(48, 80), :] = jnp.zeros((80, CHUNKS * WIDE), BF16)
 
     settle(recv1.at[pl.ds(0, 7)], small_recv.at[0])
-    found1, decays = combined(recv1, yc, power192, False)
+    settle(keep1.at[pl.ds(0, 7)], small_recv.at[3])
+    found1, decays = combined(recv1, keep1, yc, power192, False)
     for d in range(2):
         for m in range(2):
             put(msg2, d, m, found1[d][2][m])
-    put_decay(msg2, product(decays))
-    for k in (4, 3, 5, 2, 6, 1, 7):
+    dec2[0] = product(decays)[0:1, :]
+    for k in FAR:
         other, device = z_peer(k)
-        part = pl.ds(jnp.where(other > z, 0, 1), 2)
+        part = jnp.where(other > z, 0, 1)
         send(msg2.at[part], recv2.at[z, part], small_send.at[1], small_recv.at[1], device)
+        send(dec2.at[0], keep2.at[z], small_send.at[4], small_recv.at[4], device)
     recv2[pl.ds(z, 1)] = msg2[...][None]
-    settle(recv2.at[pl.ds(0, 7), pl.ds(0, 2)], small_recv.at[1])
-    found2, _ = combined(recv2, z, power1536, True)
+    keep2[pl.ds(z, 1)] = dec2[...]
+    settle(recv2.at[pl.ds(0, 7), 0], small_recv.at[1])
+    settle(keep2.at[pl.ds(0, 7)], small_recv.at[4])
+    found2, _ = combined(recv2, keep2, z, power1536, True)
     initial = []
     for d in range(2):
         pa, ps, _ = found1[d]
@@ -394,7 +396,7 @@
         middle[:, cols] = v
         rows[pl.ds(0, 48), cols] = v.astype(BF16)
         out1[:, :, cols] = dot(taken[...], rows[:, cols]).astype(BF16).reshape(8, 16, WIDE)
-        for k in range(1, 8):
+        for k in FAR:
             other, device = yc_peer(k)
             send(out1.at[other, :, cols], in1.at[yc, :, cols], yc_send.at[0], yc_recv.at[0, c], device)
         in1[pl.ds(yc, 1), :, cols] = out1[pl.ds(yc, 1), :, cols]
@@ -415,13 +417,10 @@
         send(block, xin.at[1, i, :, cols], x_send.at[0], rest if h else x_recv.at[0, i], (sp, right))
         send(block, xin.at[2, i, :, cols], x_send.at[1], x_recv.at[1, i] if h else rest, (sp, left))
 
-    def pass_on(i):
-        block = xin.at[1, i, :, side(0)]
-        settle(block, x_recv.at[0, i])
-        send(block, xin.at[3, i, :, side(0)], x_send.at[2], o_recv.at[i // 4], (sp, right))
-        block = xin.at[2, i, :, side(1)]
-        settle(block, x_recv.at[1, i])
-        send(block, xin.at[3, i, :, side(1)], x_send.at[3], o_recv.at[i // 4], (sp, left))
+    def pass_on(i, h):
+        block = xin.at[1 + h, i, :, side(h)]
+        settle(block, x_recv.at[h, i])
+        send(block, xin.at[3, i, :, side(h)], x_send.at[2 + h], o_recv.at[i // 4], (sp, (right, left)[h]))
 
     for c in range(CHUNKS):
         cols = pl.ds(WIDE * c, WIDE)
@@ -432,7 +431,7 @@
         for i in range(1, 4):
             start_z(i, c // 2, cols)
         spread(0, c // 2, cols)
-    for i in range(4, 8):
+    for i in range(4, 5):
         for h in range(2):
             start_z(i, h, side(h))
 
@@ -449,30 +448,29 @@
         cols = pl.ds(WIDE * c, WIDE)
         part = dot(hidden[g], w_down[:, cols]).reshape(4, 4, 16, WIDE)
         opp_out[g, :, :, cols] = part[3].astype(BF16)
-        send(opp_out.at[g, low, :, cols], fwd_r.at[g, :, :, cols], rs_send.at[0], rs_recv.at[0, g, c], (sp, right))
-        send(opp_out.at[g, high, :, cols], fwd_l.at[g, :, :, cols], rs_send.at[1], rs_recv.at[1, g, c], (sp, left))
+        send(opp_out.at[g, low, :, cols], fwd.at[0, g, :, :, cols], rs_send.at[0], rs_recv.at[0, g, c], (sp, right))
+        send(opp_out.at[g, high, :, cols], fwd.at[1, g, :, :, cols], rs_send.at[1], rs_recv.at[2, g, c], (sp, left))
         right_out[g, high, :, cols] = part[2, 2:4].astype(BF16)
         keep_r[g, :, :, cols] = part[2, 0:2]
-        send(right_out.at[g, high, :, cols], from_l.at[g, high, :, cols], rs_send.at[2], rs_recv.at[2, g, c], (sp, right))
+        send(right_out.at[g, high, :, cols], sums.at[0, g, high, :, cols], rs_send.at[2], rs_recv.at[1, g, c], (sp, right))
         left_out[g, low, :, cols] = part[1, 0:2].astype(BF16)
         keep_l[g, :, :, cols] = part[1, 2:4]
-        send(left_out.at[g, low, :, cols], from_r.at[g, low, :, cols], rs_send.at[3], rs_recv.at[3, g, c], (sp, left))
+        send(left_out.at[g, low, :, cols], sums.at[1, g, low, :, cols], rs_send.at[3], rs_recv.at[1, g, c], (sp, left))
         keep_o[g, :, :, cols] = part[0]
 
     def add_on(g, c):
         cols = pl.ds(WIDE * c, WIDE)
-        settle(fwd_r.at[g, :, :, cols], rs_recv.at[0, g, c])
-        right_out[g, low, :, cols] = (keep_r[g, :, :, cols] + fwd_r[g, :, :, cols].astype(F32)).astype(BF16)
-        send(right_out.at[g, low, :, cols], from_l.at[g, low, :, cols], rs_send.at[2], rs_recv.at[2, g, c], (sp, right))
-        settle(fwd_l.at[g, :, :, cols], rs_recv.at[1, g, c])
-        left_out[g, high, :, cols] = (keep_l[g, :, :, cols] + fwd_l[g, :, :, cols].astype(F32)).astype(BF16)
-        send(left_out.at[g, high, :, cols], from_r.at[g, high, :, cols], rs_send.at[3], rs_recv.at[3, g, c], (sp, left))
+        settle(fwd.at[0, g, :, :, cols], rs_recv.at[0, g, c])
+        right_out[g, low, :, cols] = (keep_r[g, :, :, cols] + fwd[0, g, :, :, cols].astype(F32)).astype(BF16)
+        send(right_out.at[g, low, :, cols], sums.at[0, g, low, :, cols], rs_send.at[2], rs_recv.at[1, g, c], (sp, right))
+        settle(fwd.at[1, g, :, :, cols], rs_recv.at[2, g, c])
+        left_out[g, high, :, cols] = (keep_l[g, :, :, cols] + fwd[1, g, :, :, cols].astype(F32)).astype(BF16)
+        send(left_out.at[g, high, :, cols], sums.at[1, g, high, :, cols], rs_send.at[3], rs_recv.at[1, g, c], (sp, left))
 
     def finish_sums(g, c):
         cols = pl.ds(WIDE * c, WIDE)
-        settle(from_l.at[g, :, :, cols], rs_recv.at[2, g, c])
-        settle(from_r.at[g, :, :, cols], rs_recv.at[3, g, c])
-        part = keep_o[g, :, :, cols] + from_l[g, :, :, cols].astype(F32) + from_r[g, :, :, cols].astype(F32)
+        settle(sums.at[:, g, :, :, cols], rs_recv.at[1, g, c])
+        part = keep_o[g, :, :, cols] + sums[0, g, :, :, cols].astype(F32) + sums[1, g, :, :, cols].astype(F32)
         ans[pl.ds(4 * g, 4), :, cols] = part.astype(BF16)
         for i in range(4 * g, 4 * g + 4):
             if i == 0:
@@ -485,7 +483,7 @@
         settle(b2in.at[pl.ds(0, 7), :, cols], z_back.at[c])
         moved = dot(swap[...], b2in[:, :, cols].reshape(128, WIDE)).astype(BF16)
         b2out[:, :, cols] = moved.reshape(8, 16, WIDE)
-        for k in range(1, 8):
+        for k in FAR:
             other, device = yc_peer(k)
             send(b2out.at[other, :, cols], b1in.at[yc, :, cols], yc_send.at[1], yc_recv.at[1, c], device)
         b1in[pl.ds(yc, 1), :, cols] = b2out[pl.ds(yc, 1), :, cols]
@@ -494,39 +492,48 @@
         for h in range(2):
             settle(xin.at[0, i, :, side(h)], z_recv.at[i, h])
             spread(i, h, side(h))
-        pass_on(i - 1)
+            if i == 1:
+                pass_on(0, h)
+        for later in {1: (5, 6), 2: (7,)}.get(i, ()):
+            for h in range(2):
+                start_z(later, h, side(h))
+        if i > 2:
+            pass_on(i - 2, 0)
+            pass_on(i - 2, 1)
         if i == 1:
             for n in (15, 16, 17):
                 loads[n].wait()
     multiply(0)
-    pass_on(7)
+    pass_on(6, 0)
+    pass_on(6, 1)
+    pass_on(7, 0)
+    pass_on(7, 1)
     start_sums(0, 0)
     start_sums(0, 1)
-    start_sums(0, 2)
-    add_on(0, 0)
     multiply(1)
     start_sums(1, 0)
     start_sums(1, 1)
+    add_on(0, 0)
     add_on(0, 1)
     start_sums(1, 2)
     add_on(1, 0)
     start_sums(1, 3)
     add_on(1, 1)
+    start_sums(0, 2)
+    start_sums(0, 3)
     finish_sums(0, 0)
+    add_on(1, 2)
     finish_sums(0, 1)
-    add_on(1, 2)
     finish_sums(1, 0)
     add_on(1, 3)
-    start_sums(0, 3)
     finish_sums(1, 1)
     add_on(0, 2)
     finish_sums(1, 2)
     add_on(0, 3)
     finish_sums(1, 3)
-    go_home(0)
     finish_sums(0, 2)
     finish_sums(0, 3)
-    for c in range(1, CHUNKS):
+    for c in range(CHUNKS):
         go_home(c)
 
     total = jnp.zeros((48, 1), F32)
@@ -549,15 +556,17 @@
         out[:, cols] = (middle[:, cols] - mean) * factor
 
     settle(recv1.at[pl.ds(0, 7)], small_send.at[0])
-    settle(recv2.at[pl.ds(0, 7), pl.ds(0, 2)], small_send.at[1])
+    settle(recv2.at[pl.ds(0, 7), 0], small_send.at[1])
+    settle(keep1.at[pl.ds(0, 7)], small_send.at[3])
+    settle(keep2.at[pl.ds(0, 7)], small_send.at[4])
     settle(act_in.at[pl.ds(0, 3)], small_send.at[2])
     for index in range(2):
         settle(out1.at[pl.ds(0, 7)], yc_send.at[index])
         settle(out2.at[pl.ds(0, 7)], z_send.at[index])
         settle(xin.at[0], x_send.at[index])
         settle(xin.at[0, pl.ds(0, 4)], x_send.at[2 + index])
-        settle(fwd_r, rs_send.at[index])
-        settle(from_l, rs_send.at[2 + index])
+        settle(fwd.at[0], rs_send.at[index])
+        settle(sums.at[0], rs_send.at[2 + index])
 
 
 def on_device(
@@ -568,7 +577,6 @@
     dma = pltpu.SemaphoreType.DMA
     slab = pltpu.VMEM((8, 16, 2048), BF16)
     groups = pltpu.VMEM((2, 4, 16, 2048), BF16)
-    half = pltpu.VMEM((2, 2, 16, 2048), BF16)
     normed = pl.pallas_call(
         kernel,
         out_shape=jax.ShapeDtypeStruct((48, 2048), F32),
@@ -578,10 +586,14 @@
         + [
             pltpu.VMEM((4, 192, 128), F32),
             pltpu.VMEM((4, 4, 192, 128), F32),
-            pltpu.VMEM((3, 8, 128), F32),
-            pltpu.VMEM((8, 3, 8, 128), F32),
-            pltpu.VMEM((3, 8, 128), F32),
-            pltpu.VMEM((8, 3, 8, 128), F32),
+            pltpu.VMEM((2, 8, 128), F32),
+            pltpu.VMEM((8, 2, 8, 128), F32),
+            pltpu.VMEM((2, 8, 128), F32),
+            pltpu.VMEM((8, 2, 8, 128), F32),
+            pltpu.VMEM((1, 1, 512), F32),
+            pltpu.VMEM((8, 1, 512), F32),
+            pltpu.VMEM((1, 1, 512), F32),
+            pltpu.VMEM((8, 1, 512), F32),
             pltpu.VMEM((4, 48, 128), BF16),
             pltpu.VMEM((4, 48, 128), BF16),
             pltpu.VMEM((48, 2048), F32),
@@ -593,16 +605,18 @@
             slab, slab, slab,
             pltpu.VMEM((4, 8, 16, 2048), BF16),
             pltpu.VMEM((2, 256, 256), BF16),
-            groups, half, half,
-            groups, groups, groups, groups,
+            groups,
+            pltpu.VMEM((2, 2, 2, 16, 2048), BF16),
+            groups, groups,
+            pltpu.VMEM((2, 2, 4, 16, 2048), BF16),
             pltpu.VMEM((2, 2, 16, 2048), F32),
             pltpu.VMEM((2, 2, 16, 2048), F32),
             pltpu.VMEM((2, 4, 16, 2048), F32),
             slab, slab, slab, slab,
-            dma((len(INPUTS),)), dma((3,)), dma((3,)),
+            dma((len(INPUTS),)), dma((5,)), dma((5,)),
             dma((2,)), dma((2, CHUNKS)), dma((2,)), dma((8, 2)), dma((CHUNKS,)),
             dma((4,)), dma((2, 8)), dma((2,)),
-            dma((4,)), dma((4, 2, CHUNKS)),
+            dma((4,)), dma((3, 2, CHUNKS)),
         ],
         compiler_params=pltpu.CompilerParams(
             collective_id=0, has_side_effects=True, vmem_limit_bytes=40 * 1024 * 1024

time: 83.4 us -> 81.1 us (0.972)
  Pallas kernels: 82.6 us -> 80.3 us
    pallas_call x1, Pallas kernels: 82.6 us -> 80.3 us  [on_device(): pl.pallas_call(kernel, out_shape=jax.ShapeDtypeStruct((48, 2048), F32), i...]
where the time goes in v2:
time: 81.1 us; the launch traced here: 81 us
  Pallas kernels  80.3 us (99%)
    pallas_call x1, Pallas kernels, on_device(): pl.pallas_call(kernel, out_shape=jax.ShapeDtypeStruct((48, 2048), F32), i...  80.3 us

profile of v2, /device:TPU:1, one launch (start us, length us, event | category | flops | bytes accessed | tf_op | source)
XLA Modules:
  0.0 81.0 jit_solution(9596025110064634844)
XLA Ops:
  0.0 0.0 copy-start
  0.0 80.3 %layer.1 = f32[48,2048]{1,0:T(8,128)S(1)} custom-call(bf16[48,2048]{1,0:T(8,128)(2,1)} %refs_0_.1, bf16[192,128]{1,0:T(8,128)(2,1)} %refs_1_.1, f32[8,192]{1,0:T(8,128)} %bitcast.20, f32[2,8,64]{2,1,0:T(8,128)} %refs_3_.1, f32[2,8,64]{2,1,0:T(8,128)} %refs_4_.1, f32[256,64]{1,0:T(8,128)} %bitcast.16, f32[256,64]{1,0:T(8,128)} %bitcast.17, ...), custom_call_target="tpu_custom_call" | custom-call | tf_op jit(solution)/shard_map/layer/pallas_call | solution.py:580
  80.3 0.0 copy-done
  80.3 0.7 multiply_convert_fusion
Async XLA Ops:
  0.0 80.3 %copy-start = (f32[2048]{0:T(1024)S(1)}, f32[2048]{0:T(1024)}, u32[]{:S(2)}) copy-start(f32[2048]{0:T(1024)} %param.31) | copy-start | bytes 24580

commit v3 on v2

--- a/solution.py
+++ b/solution.py
@@ -494,12 +494,13 @@
             spread(i, h, side(h))
             if i == 1:
                 pass_on(0, h)
-        for later in {1: (5, 6), 2: (7,)}.get(i, ()):
+        for later in {1: (5,), 2: (6,), 3: (7,)}.get(i, ()):
             for h in range(2):
                 start_z(later, h, side(h))
-        if i > 2:
-            pass_on(i - 2, 0)
-            pass_on(i - 2, 1)
+        passed = {2: 1, 3: 2, 5: 3, 6: 4, 7: 5}.get(i)
+        if passed is not None:
+            pass_on(passed, 0)
+            pass_on(passed, 1)
         if i == 1:
             for n in (15, 16, 17):
                 loads[n].wait()

time: 81.1 us -> 81.1 us (level)
  no operation moved by 1% of the time
where the time goes in v3:
time: 81.1 us; the launch traced here: 81 us
  Pallas kernels  80.3 us (99%)
    pallas_call x1, Pallas kernels, on_device(): pl.pallas_call(kernel, out_shape=jax.ShapeDtypeStruct((48, 2048), F32), i...  80.3 us

profile of v3, /device:TPU:1, one launch (start us, length us, event | category | flops | bytes accessed | tf_op | source)
XLA Modules:
  0.0 81.0 jit_solution(13458355869657551007)
XLA Ops:
  0.0 0.0 copy-start
  0.0 80.3 %layer.1 = f32[48,2048]{1,0:T(8,128)S(1)} custom-call(bf16[48,2048]{1,0:T(8,128)(2,1)} %refs_0_.1, bf16[192,128]{1,0:T(8,128)(2,1)} %refs_1_.1, f32[8,192]{1,0:T(8,128)} %bitcast.20, f32[2,8,64]{2,1,0:T(8,128)} %refs_3_.1, f32[2,8,64]{2,1,0:T(8,128)} %refs_4_.1, f32[256,64]{1,0:T(8,128)} %bitcast.16, f32[256,64]{1,0:T(8,128)} %bitcast.17, ...), custom_call_target="tpu_custom_call" | custom-call | tf_op jit(solution)/shard_map/layer/pallas_call | solution.py:581
  80.3 0.0 copy-done
  80.3 0.7 multiply_convert_fusion
Async XLA Ops:
  0.0 80.3 %copy-start = (f32[2048]{0:T(1024)S(1)}, f32[2048]{0:T(1024)}, u32[]{:S(2)}) copy-start(f32[2048]{0:T(1024)} %param.31) | copy-start | bytes 24580
